TPU v7x, 32 devices: a whole 2x2x4 slice. The times are simulated.
32 devices in a mesh: grp: 2 (over x), tp: 16 (over z, y, core).
Axes of the slice: x: 2, y: 2, z: 4, core: 2. Of those that a mesh axis runs over, the one named last changes fastest.
Arguments:
- residual_channel: bfloat16 [256, 8, 4096], P('grp', None, 'tp'), parts along dimension 0, may hold values from -18 to 18, as said below
- prior_block_multiplier: float32 [2, 4096], replicated, may hold values from 0.1 to 1.9
- probe_map_matrix: bfloat16 [2, 4096, 2048], P(None, None, 'tp'), may hold values from -0.09375 to 0.09375
- lookup_map_matrix: bfloat16 [2, 4096, 2048], P(None, None, 'tp'), may hold values from -0.09375 to 0.09375
- content_map_matrix: bfloat16 [2, 4096, 2048], P(None, None, 'tp'), may hold values from -0.09375 to 0.09375
- emission_valve_matrix: bfloat16 [2, 4096, 2048], P(None, None, 'tp'), may hold values from -0.09375 to 0.09375
- forgetting_map_matrix: bfloat16 [2, 4096, 32], replicated, may hold values from -0.09375 to 0.09375
- insertion_rate_matrix: bfloat16 [2, 4096, 32], replicated, may hold values from -0.09375 to 0.09375
- forgetting_magnitude_exponent: float32 [2, 32], P(None, 'tp'), may hold values from -4.6 to -1.2
- channel_forgetting_offset: float32 [2, 32], P(None, 'tp'), may hold values from -2 to 1
- surplus_forgetting_amounts: float32 [2, 256, 8, 32], P(None, 'grp', None, 'tp'), parts along dimension 1, may hold values from -0.7 to 0
- readout_rescale_multiplier: float32 [2, 2048], P(None, 'tp'), may hold values from 0.1 to 1.9
- emission_map_matrix: bfloat16 [2, 2048, 4096], P(None, None, 'tp'), may hold values from -2 to 2
- post_mixing_multiplier: float32 [2, 4096], replicated, may hold values from 0.1 to 1.9
- recurrent_matrices: float32 [2, 256, 32, 4096], P(None, 'grp', 'tp'), parts along dimension 1, may hold values from -6 to 6
Outputs:
- new_stream: bfloat16 [256, 8, 4096], P('grp', None, 'tp'), parts along dimension 0
- new_memory: float32 [2, 256, 32, 4096], P(None, 'grp', 'tp'), parts along dimension 1
There are 2 independent parts, one for each index of `grp`. A program takes and returns all parts, laid end to end along the dimension named above; an argument that names none is the same for every part. Nothing has to cross between parts.
Inputs may be any that keep to these rules, and one draw needn't show every extreme that they name: `residual_channel`: column scales of the features differ widely.
All inputs are finite; a program needn't handle non-finite values.
Results may differ from a plain program's by a relative error of at most 0.0081.
Values may be sent and summed in bfloat16 or wider, within the bound.
No kernel may reach another device: no remote copies, remote signals or barrier semaphores. Data moves between devices by JAX's collectives and lax.ppermute only.
A program may use at most 192 MiB of HBM per device.

v0:
```python
import jax
import jax.numpy as jnp
from jax import lax
from jax.sharding import PartitionSpec as P

D = 4096
HEAD_DIM = 64
LAYERS = 2


EPS = 1e-06
HIGH = lax.Precision.HIGHEST


def solve_lower(a_mat, right_side):
    length = right_side.shape[-2]
    solved_rows = []
    for row_at in range(length):
        current_row = right_side[..., row_at, :]
        for col_at in range(row_at):
            current_row = current_row - a_mat[..., row_at, col_at][..., None] * solved_rows[col_at]
        solved_rows.append(current_row)
    return jnp.stack(solved_rows, axis=-2)


def delta_block(queries, key_rows, values, forgetting_exponent_amount, strength, matrix_state):
    length = queries.shape[2]
    causal = jnp.tril(jnp.ones((length, length), bool))
    strict = jnp.tril(jnp.ones((length, length), bool), -1)
    cumulative = jnp.cumsum(forgetting_exponent_amount, axis=-1)
    decay_mat = jnp.where(
        causal,
        jnp.exp(jnp.where(causal, cumulative[..., :, None] - cumulative[..., None, :], 0.0)),
        0.0,
    )
    key_gram = jnp.einsum("bhtd,bhsd->bhts", key_rows, key_rows, precision=HIGH)
    a_mat = jnp.where(strict, strength[..., :, None] * decay_mat * key_gram, 0.0)
    right_side = jnp.concatenate(
        [strength[..., None] * values, (strength * jnp.exp(cumulative))[..., None] * key_rows],
        axis=-1,
    )
    solved = solve_lower(a_mat, right_side)
    width_v = values.shape[-1]
    update = solved[..., :width_v] - jnp.einsum(
        "bhtk,bhkv->bhtv", solved[..., width_v:], matrix_state, precision=HIGH
    )
    scores = jnp.einsum("bhtd,bhsd->bhts", queries, key_rows, precision=HIGH) * decay_mat
    output = jnp.exp(cumulative)[..., None] * jnp.einsum(
        "bhtk,bhkv->bhtv", queries, matrix_state, precision=HIGH
    )
    output = output + jnp.einsum("bhts,bhsv->bhtv", scores, update, precision=HIGH)
    final_log = cumulative[..., -1:]
    revised_memory_matrix = jnp.exp(final_log)[..., None] * matrix_state + jnp.einsum(
        "bhsk,bhsv->bhkv",
        key_rows * jnp.exp(final_log - cumulative)[..., None],
        update,
        precision=HIGH,
    )
    return (output, revised_memory_matrix)


def unit_rows(matrix):
    return matrix * lax.rsqrt(jnp.sum(matrix * matrix, axis=-1, keepdims=True) + EPS)


def token_blender(
    mapped_token_vectors,
    magnitude_exponent,
    offset_terms_array,
    surplus_forgetting_exponent,
    multiplier_terms_array,
    incoming_memory_matrix,
    batch_total,
    generation_round_total,
):
    rounded = [
        lax.optimization_barrier(part_sum.astype(jnp.bfloat16)).astype(jnp.float32)
        for part_sum in mapped_token_vectors
    ]
    queries, keys_raw, values_raw, gate_raw, decay_pre, strength_pre = rounded
    head_count = incoming_memory_matrix.shape[1]

    def to_heads(matrix):
        return matrix.reshape(batch_total, generation_round_total, head_count, HEAD_DIM).transpose(
            0, 2, 1, 3
        )

    def per_head(matrix):
        return matrix.reshape(batch_total, generation_round_total, head_count).transpose(0, 2, 1)

    queries = unit_rows(jax.nn.silu(to_heads(queries))) * HEAD_DIM ** (-0.5)
    key_rows = unit_rows(jax.nn.silu(to_heads(keys_raw)))
    values = jax.nn.silu(to_heads(values_raw))
    forgetting_exponent_amount = -jnp.exp(magnitude_exponent)[None, :, None] * jax.nn.softplus(
        per_head(decay_pre) + offset_terms_array[None, :, None]
    )
    forgetting_exponent_amount = forgetting_exponent_amount + surplus_forgetting_exponent.transpose(
        0, 2, 1
    )
    strength = jax.nn.sigmoid(per_head(strength_pre))
    matrix_state = incoming_memory_matrix.reshape(batch_total, head_count, HEAD_DIM, HEAD_DIM)
    output, revised_memory_matrix = delta_block(
        queries, key_rows, values, forgetting_exponent_amount, strength, matrix_state
    )
    normed = output * lax.rsqrt(jnp.mean(output * output, axis=-1, keepdims=True) + EPS)
    normed = (
        normed
        * multiplier_terms_array.reshape(head_count, HEAD_DIM)[None, :, None, :]
        * jax.nn.silu(to_heads(gate_raw))
    )
    blended_token_vectors = (
        normed.transpose(0, 2, 1, 3)
        .reshape(batch_total * generation_round_total, head_count * HEAD_DIM)
        .astype(jnp.bfloat16)
    )
    return (
        blended_token_vectors,
        revised_memory_matrix.reshape(batch_total, head_count, HEAD_DIM * HEAD_DIM),
    )


def project(portion, weights):
    return tuple(
        (jnp.dot(portion, weight, preferred_element_type=jnp.float32) for weight in weights)
    )


def out_project(blended_token_vectors, weight_rows):
    return jnp.dot(
        lax.all_gather(blended_token_vectors, "tp", axis=1, tiled=True),
        weight_rows,
        preferred_element_type=jnp.float32,
    ).astype(jnp.bfloat16)


def post_residual(widened, mixed_out, multiplier_terms_array, complete):
    mixed_wide = lax.optimization_barrier(mixed_out).astype(jnp.float32)
    squares = jnp.sum(mixed_wide * mixed_wide, axis=-1)
    if not complete:
        squares = lax.psum(squares, "tp")
    post_rms = lax.rsqrt(squares / D + EPS)[:, None]
    return lax.optimization_barrier(
        (widened + mixed_wide * post_rms * multiplier_terms_array).astype(jnp.bfloat16)
    )


def local(
    residual_channel,
    prior_block_multiplier,
    probe_map_matrix,
    lookup_map_matrix,
    content_map_matrix,
    emission_valve_matrix,
    forgetting_map_matrix,
    insertion_rate_matrix,
    forgetting_magnitude_exponent,
    channel_forgetting_offset,
    surplus_forgetting_amounts,
    readout_rescale_multiplier,
    emission_map_matrix,
    post_mixing_multiplier,
    recurrent_matrices,
):
    batch_total, generation_round_total, own_width = residual_channel.shape
    head_count = recurrent_matrices.shape[2]
    row_count = batch_total * generation_round_total
    col_offset = lax.axis_index("tp") * own_width
    head_offset = lax.axis_index("tp") * head_count
    new_states = []

    def mix_layer(mapped_token_vectors, block_index_number):
        blended_token_vectors, revised_memory_matrix = token_blender(
            mapped_token_vectors,
            forgetting_magnitude_exponent[block_index_number],
            channel_forgetting_offset[block_index_number],
            surplus_forgetting_amounts[block_index_number],
            readout_rescale_multiplier[block_index_number],
            recurrent_matrices[block_index_number],
            batch_total,
            generation_round_total,
        )
        new_states.append(revised_memory_matrix)
        return out_project(blended_token_vectors, emission_map_matrix[block_index_number])

    def own_cols(matrix):
        return lax.dynamic_slice_in_dim(matrix, col_offset, own_width, matrix.ndim - 1)

    whole_rows = lax.all_gather(
        residual_channel.reshape(row_count, own_width), "tp", axis=1, tiled=True
    )
    current = whole_rows
    for block_index_number in range(LAYERS):
        widened = whole_rows.astype(jnp.float32)
        inv_rms = lax.rsqrt(jnp.mean(widened * widened, axis=-1, keepdims=True) + EPS)
        hidden = (widened * inv_rms * prior_block_multiplier[block_index_number]).astype(
            jnp.bfloat16
        )
        weights = (
            probe_map_matrix[block_index_number],
            lookup_map_matrix[block_index_number],
            content_map_matrix[block_index_number],
            emission_valve_matrix[block_index_number],
            lax.dynamic_slice_in_dim(
                forgetting_map_matrix[block_index_number], head_offset, head_count, 1
            ),
            lax.dynamic_slice_in_dim(
                insertion_rate_matrix[block_index_number], head_offset, head_count, 1
            ),
        )
        mapped_token_vectors = project(hidden, weights)
        mixed_out = mix_layer(mapped_token_vectors, block_index_number)
        if block_index_number < LAYERS - 1:
            gathered = lax.all_gather(mixed_out, "tp", axis=1, tiled=True)
            whole_rows = post_residual(
                widened, gathered, post_mixing_multiplier[block_index_number], True
            )
        else:
            current = post_residual(
                own_cols(widened),
                mixed_out,
                own_cols(post_mixing_multiplier[block_index_number]),
                False,
            )
    return (
        current.reshape(batch_total, generation_round_total, own_width),
        jnp.stack(new_states, axis=0),
    )


def solution(mesh):
    return jax.shard_map(
        local,
        mesh=mesh,
        in_specs=(
            P("grp", None, "tp"),
            P(),
            P(None, None, "tp"),
            P(None, None, "tp"),
            P(None, None, "tp"),
            P(None, None, "tp"),
            P(),
            P(),
            P(None, "tp"),
            P(None, "tp"),
            P(None, "grp", None, "tp"),
            P(None, "tp"),
            P(None, None, "tp"),
            P(),
            P(None, "grp", "tp", None),
        ),
        out_specs=(P("grp", None, "tp"), P(None, "grp", "tp", None)),
        check_vma=False,
    )
```

profile of v0, /device:TPU:0, one launch (start us, length us, event | category | flops | bytes accessed | tf_op | source)
XLA Modules:
  0.0 673.6 jit_solution(834577331812609737)
XLA Ops:
  11.3 14.3 %fusion.190 = (f32[1,128,2,4096]{3,2,1,0:T(2,128)}, f32[1,128,2,4096]{3,2,1,0:T(2,128)}) fusion(f32[2,128,2,4096]{3,2,1,0:T(2,128)} %param.29), kind=kLoop, calls=%fused_computation.324 | loop fusion | bytes 16777216 | tf_op jit(solution)/shard_map/slice | solution.py:178
  25.6 7.4 %copy.607 = f32[1,128,2,4096]{1,3,2,0:T(8,128)} copy(f32[1,128,2,4096]{3,2,1,0:T(2,128)} %get-tuple-element.41) | data formatting | bytes 8388608
  33.1 9.3 %copy.482 = f32[128,2,64,64]{3,2,1,0:T(8,128)} copy(f32[128,2,64,64]{0,3,2,1:T(8,128)} %bitcast.322) | data formatting | bytes 8388608 | tf_op jit(solution)/shard_map/reshape;squeeze | solution.py:101
  44.6 46.0 %all-gather.5.cloned.1.call-done = bf16[1024,4096]{1,0:T(8,128)(2,1)} async-done(((bf16[1024,256]{1,0:T(8,128)(2,1)}), bf16[1024,4096]{1,0:T(8,128)(2,1)}) %all-gather.5.cloned.1.call-update) | async-done | bytes 8388624 | tf_op jit(solution)/shard_map/all_gather | solution.py:188
  95.7 10.5 %fusion.4 = bf16[1024,4096]{1,0:T(8,128)(2,1)} fusion(bf16[1024,4096]{1,0:T(8,128)(2,1)} %all-gather.5.cloned.1.call-done, f32[4096]{0:T(1024)S(1)} %bitcast.336, f32[1024]{0:T(1024)S(1)} %add_rsqrt_fusion.7), kind=kLoop, calls=%fused_computation.9 | loop fusion | flops 16777216 | bytes 16797696 | tf_op jit(solution)/shard_map/convert_element_type | solution.py:195
  211.4 7.5 %fusion.72 = f32[128,2,8,64]{3,2,1,0:T(8,128)S(1)} fusion(f32[128,2,64,64]{3,2,1,0:T(8,128)S(1)} %bitcast.315, f32[128,2,8,64]{3,0,2,1:T(8,128)S(1)} %multiply_multiply_fusion.1), kind=kOutput, calls=%fused_computation.126 | convolution fusion | flops 100663296 | bytes 5242880 | tf_op jit(solution)/shard_map/bhtk,bhkv->bhtv/dot_general | solution.py:48
  218.9 7.2 %fusion.46 = f32[128,2,8,64]{3,2,1,0:T(8,128)S(1)} fusion(f32[128,2,64,64]{3,2,1,0:T(8,128)S(1)} %bitcast.315, f32[128,2,8,64]{3,0,2,1:T(8,128)S(1)} %slice.467), kind=kOutput, calls=%fused_computation.90 | convolution fusion | flops 100663296 | bytes 5242880 | tf_op jit(solution)/shard_map/bhtk,bhkv->bhtv/dot_general | solution.py:44
  237.5 50.8 %all-gather.7.cloned.1.call-done = bf16[1024,2048]{1,0:T(8,128)(2,1)} async-done(((bf16[1024,128]{1,0:T(8,128)(2,1)}), bf16[1024,2048]{1,0:T(8,128)(2,1)}) %all-gather.7.cloned.1.call-update) | async-done | bytes 4194320 | tf_op jit(solution)/shard_map/all_gather | solution.py:130
  293.7 7.4 %copy.609 = f32[1,128,2,4096]{1,3,2,0:T(8,128)} copy(f32[1,128,2,4096]{3,2,1,0:T(2,128)} %get-tuple-element.40) | data formatting | bytes 8388608
  301.1 9.1 %copy.539 = f32[128,2,64,64]{3,2,1,0:T(8,128)} copy(f32[128,2,64,64]{0,3,2,1:T(8,128)} %bitcast.323) | data formatting | bytes 8388608 | tf_op jit(solution)/shard_map/reshape;squeeze | solution.py:101
  310.8 58.1 %all-gather.9.cloned.1.call-done = bf16[1024,4096]{1,0:T(8,128)(2,1)} async-done(((bf16[1024,256]{1,0:T(8,128)(2,1)}), bf16[1024,4096]{1,0:T(8,128)(2,1)}) %all-gather.9.cloned.1.call-update) | async-done | bytes 8388624 | tf_op jit(solution)/shard_map/all_gather | solution.py:213
  374.7 6.9 %fusion.5 = bf16[1024,4096]{1,0:T(8,128)(2,1)S(1)} fusion(bf16[1024,4096]{1,0:T(8,128)(2,1)S(1)} %copy-done.1, bf16[1024,4096]{1,0:T(8,128)(2,1)} %all-gather.5.cloned.1.call-done, f32[4096]{0:T(1024)S(1)} %bitcast.334, f32[1024]{0:T(1024)S(1)} %add_rsqrt_fusion.6), kind=kLoop, calls=%fused_computation.10 | loop fusion | flops 25165824 | bytes 25186304 | tf_op jit(solution)/shard_map/convert_element_type | solution.py:143
  386.6 10.4 %multiply_convert_fusion = bf16[1024,4096]{1,0:T(8,128)(2,1)} fusion(f32[4096]{0:T(1024)S(1)} %bitcast.335, f32[1024]{0:T(1024)S(1)} %add_rsqrt_fusion.5, bf16[1024,4096]{1,0:T(8,128)(2,1)} %copy-done), kind=kLoop, calls=%fused_computation.11 | loop fusion | flops 16777216 | bytes 16797696 | tf_op jit(solution)/shard_map/convert_element_type | solution.py:195
  411.2 6.8 %convolution_convert_fusion.2 = bf16[1024,128]{1,0:T(8,128)(2,1)} fusion(bf16[1024,4096]{1,0:T(8,128)(2,1)} %multiply_convert_fusion, bf16[2,4096,128]{2,1,0:T(8,128)(2,1)} %param.20), kind=kOutput, calls=%fused_computation.26 | convolution fusion | flops 1073872896 | bytes 9699328 | tf_op jit(solution)/shard_map/dot_general | solution.py:124
  464.3 10.4 %fusion.64 = f32[128,2,8,64]{3,2,1,0:T(8,128)} fusion(f32[128,2,64,64]{3,2,1,0:T(8,128)} %copy.539, f32[128,2,8,64]{3,0,2,1:T(8,128)S(1)} %copy-done.9), kind=kOutput, calls=%fused_computation.118 | convolution fusion | flops 100663296 | bytes 5242880 | tf_op jit(solution)/shard_map/bhtk,bhkv->bhtv/dot_general | solution.py:48
  523.9 7.2 %fusion.44 = f32[128,2,8,64]{3,2,1,0:T(8,128)S(1)} fusion(f32[128,2,64,64]{3,2,1,0:T(8,128)S(1)} %bitcast.317, f32[128,2,8,64]{3,0,2,1:T(8,128)S(1)} %slice.511), kind=kOutput, calls=%fused_computation.88 | convolution fusion | flops 100663296 | bytes 5242880 | tf_op jit(solution)/shard_map/bhtk,bhkv->bhtv/dot_general | solution.py:44
  543.0 18.4 %multiply_add_fusion.1 = f32[128,2,64,64]{3,2,1,0:T(8,128)} fusion(f32[128,2,64,64]{3,2,1,0:T(8,128)} %copy.482, f32[128,2]{1,0:T(8,128)S(1)} %bitcast.332, f32[128,2,8,64]{3,0,2,1:T(8,128)S(1)} %get-tuple-element.12, f32[128,2,8,64]{3,0,2,1:T(8,128)S(1)} %slice_subtract_fusion.1), kind=kOutput, calls=%fused_computation.15 | convolution fusion | flops 102760448 | bytes 9438208 | tf_op jit(solution)/shard_map/bhsk,bhsv->bhkv/dot_general | solution.py:53
  561.4 8.0 %copy.596 = f32[128,2,64,64]{0,3,2,1:T(8,128)} copy(f32[128,2,64,64]{3,2,1,0:T(8,128)} %multiply_add_fusion.1) | data formatting | bytes 8388608 | tf_op jit(solution)/shard_map/add | solution.py:53
  569.4 11.6 %convert_element_type.108 = f32[1024,4096]{1,0:T(8,128)} convert(bf16[1024,4096]{1,0:T(8,128)(2,1)} %copy-done) | non-fusion elementwise | flops 4194304 | bytes 25165824 | tf_op jit(solution)/shard_map/convert_element_type | solution.py:193
  582.0 18.6 %multiply_add_fusion = f32[128,2,64,64]{3,2,1,0:T(8,128)} fusion(f32[128,2,64,64]{3,2,1,0:T(8,128)} %copy.539, f32[128,2]{1,0:T(8,128)S(1)} %bitcast.333, f32[128,2,8,64]{3,0,2,1:T(8,128)S(1)} %copy-done.2, f32[128,2,8,64]{3,0,2,1:T(8,128)S(1)} %copy-done.4), kind=kOutput, calls=%fused_computation.14 | convolution fusion | flops 102760448 | bytes 9438208 | tf_op jit(solution)/shard_map/bhsk,bhsv->bhkv/dot_general | solution.py:53
  600.6 8.0 %copy.602 = f32[128,2,64,64]{0,3,2,1:T(8,128)} copy(f32[128,2,64,64]{3,2,1,0:T(8,128)} %multiply_add_fusion) | data formatting | bytes 8388608 | tf_op jit(solution)/shard_map/add | solution.py:53
  608.6 7.4 %pad_maximum_fusion = f32[2,128,2,4096]{1,3,2,0:T(8,128)} fusion(f32[1,128,2,4096]{1,3,2,0:T(8,128)} %bitcast.325, f32[1,128,2,4096]{1,3,2,0:T(8,128)} %bitcast.324), kind=kLoop, calls=%fused_computation.13 | loop fusion | flops 2097152 | bytes 16777216 | tf_op jit(solution)/shard_map/stack | solution.py:226
  616.0 13.3 %copy.603 = f32[2,128,2,4096]{3,2,1,0:T(2,128)} copy(f32[2,128,2,4096]{1,3,2,0:T(8,128)} %pad_maximum_fusion) | data formatting | bytes 16777216
  632.9 31.4 %psum.7 = f32[1024]{0:T(1024)S(1)} all-reduce(f32[1024]{0:T(1024)S(1)} %fusion.8), channel_id=1, replica_groups=mesh['grp'=2,'tp'=16] {'tp'}, use_global_device_ids=true, to_apply=%region_12.13 | all-reduce | flops 1024 | bytes 8192 | tf_op jit(solution)/shard_map/psum | solution.py:140
  (401 shorter events, 271.6 us)
Async XLA Ops:
  7.2 83.5 %all-gather.5.cloned.1.call-start = ((), (), s32[]{:S(2)}) async-start(), calls=%async_computation | async-start | bytes 8912896 | tf_op jit(solution)/shard_map/all_gather | solution.py:188
  7.9 280.4 %all-gather.7.cloned.1.call-start = ((), (), s32[]{:S(2)}) async-start(), calls=%async_computation.1 | async-start | bytes 4456448 | tf_op jit(solution)/shard_map/all_gather | solution.py:130
  33.1 10.8 %copy-start.13 = (bf16[2,4096,32]{1,2,0:T(8,128)(2,1)S(1)}, bf16[2,4096,32]{1,2,0:T(8,128)(2,1)}, u32[]{:S(2)}) copy-start(bf16[2,4096,32]{1,2,0:T(8,128)(2,1)} %param.22) | copy-start | bytes 1572868
  42.5 85.7 %copy-start.76 = (pred[8,8]{1,0:T(8,128)(4,1)}, pred[8,8]{1,0:T(8,128)(4,1)S(1)}, u32[]{:S(2)}) copy-start(pred[8,8]{1,0:T(8,128)(4,1)S(1)} %get-tuple-element.131) | copy-start | bytes 196
  42.5 85.7 %copy-start.77 = (pred[8,8]{1,0:T(8,128)(4,1)}, pred[8,8]{1,0:T(8,128)(4,1)S(1)}, u32[]{:S(2)}) copy-start(pred[8,8]{1,0:T(8,128)(4,1)S(1)} %get-tuple-element.130) | copy-start | bytes 196
  127.5 12.8 %slice-start.4 = ((s8[8388608]{0:T(1024)(128)(4,1)}), s8[4194304]{0:T(1024)(128)(4,1)S(1)}, s32[]{:S(2)}) async-start(s8[8388608]{0:T(1024)(128)(4,1)} %bitcast.318), calls=%async_computation.8 | async-start | bytes 8388608
  129.2 11.2 %slice-start.5 = ((s8[8388608]{0:T(1024)(128)(4,1)}), s8[4194304]{0:T(1024)(128)(4,1)S(1)}, s32[]{:S(2)}) async-start(s8[8388608]{0:T(1024)(128)(4,1)} %bitcast.318), calls=%async_computation.9 | async-start | bytes 8388608
  129.2 11.2 %copy-start.81 = (bf16[2,4096,128]{2,1,0:T(8,128)(2,1)S(1)}, bf16[2,4096,128]{2,1,0:T(8,128)(2,1)}, u32[]{:S(2)}) copy-start(bf16[2,4096,128]{2,1,0:T(8,128)(2,1)} %param.20) | copy-start | bytes 6291460
  232.8 60.1 %copy-start.80 = (f32[128]{0:T(128)S(1)}, f32[128]{0:T(128)}, u32[]{:S(2)}) copy-start(f32[128]{0:T(128)} %get-tuple-element.10) | copy-start | bytes 1540
  232.8 60.7 %copy-start.26 = (f32[1,128,8,2]{1,3,2,0:T(2,128)S(1)}, f32[1,128,8,2]{1,3,2,0:T(2,128)}, u32[]{:S(2)}) copy-start(f32[1,128,8,2]{1,3,2,0:T(2,128)} %get-tuple-element.119) | copy-start | bytes 24580
  237.5 131.4 %all-gather.9.cloned.1.call-start = ((), (), s32[]{:S(2)}) async-start(), calls=%async_computation.2 | async-start | bytes 8912896 | tf_op jit(solution)/shard_map/all_gather | solution.py:213
  292.9 336.4 %all-gather.11.cloned.1.call-start = ((), (), s32[]{:S(2)}) async-start(), calls=%async_computation.3 | async-start | bytes 4456448 | tf_op jit(solution)/shard_map/all_gather | solution.py:130
  397.1 12.4 %copy-start.73 = (f32[2]{0:T(128)S(1)}, f32[2]{0:T(128)}, u32[]{:S(2)}) copy-start(f32[2]{0:T(128)} %get-tuple-element.122) | copy-start | bytes 28
  397.1 12.4 %copy-start.74 = (f32[2]{0:T(128)S(1)}, f32[2]{0:T(128)}, u32[]{:S(2)}) copy-start(f32[2]{0:T(128)} %get-tuple-element.129) | copy-start | bytes 28
  410.5 23.3 %copy-start.21 = (f32[128,2,8]{2,1,0:T(2,128)}, f32[128,2,8]{2,1,0:T(2,128)S(1)}, u32[]{:S(2)}) copy-start(f32[128,2,8]{2,1,0:T(2,128)S(1)} %copy.544) | copy-start | bytes 24580
  411.2 13.4 %slice-start.6 = ((s8[8388608]{0:T(1024)(128)(4,1)}), s8[4194304]{0:T(1024)(128)(4,1)S(1)}, s32[]{:S(2)}) async-start(s8[8388608]{0:T(1024)(128)(4,1)} %bitcast.320), calls=%async_computation.10 | async-start | bytes 8388608
  434.7 11.7 %copy-start.18 = (f32[128,8,2]{1,0,2:T(8,128)S(1)}, f32[128,8,2]{1,0,2:T(8,128)}, u32[]{:S(2)}) copy-start(f32[128,8,2]{1,0,2:T(8,128)} %get-tuple-element.106) | copy-start | bytes 24580
  434.7 11.7 %copy-start.17 = (f32[128,2,8]{2,0,1:T(8,128)S(1)}, f32[128,2,8]{2,0,1:T(8,128)}, u32[]{:S(2)}) copy-start(f32[128,2,8]{2,0,1:T(8,128)} %get-tuple-element.107) | copy-start | bytes 24580
  434.7 12.4 %copy-start.16 = (f32[128,2,8]{2,0,1:T(8,128)S(1)}, f32[128,2,8]{2,0,1:T(8,128)}, u32[]{:S(2)}) copy-start(f32[128,2,8]{2,0,1:T(8,128)} %get-tuple-element.109) | copy-start | bytes 24580
  531.1 11.0 %copy-start.14 = (f32[128,2,1]{2,0,1:T(8,128)S(1)}, f32[128,2,1]{2,0,1:T(8,128)}, u32[]{:S(2)}) copy-start(f32[128,2,1]{2,0,1:T(8,128)} %get-tuple-element.102) | copy-start | bytes 3076
  569.4 11.7 %copy-start.15 = (f32[128,2,1]{2,0,1:T(8,128)S(1)}, f32[128,2,1]{2,0,1:T(8,128)}, u32[]{:S(2)}) copy-start(f32[128,2,1]{2,0,1:T(8,128)} %get-tuple-element.104) | copy-start | bytes 3076
  569.4 12.5 %copy-start.2 = (f32[128,2,8,64]{3,0,2,1:T(8,128)S(1)}, f32[128,2,8,64]{3,0,2,1:T(8,128)}, u32[]{:S(2)}) copy-start(f32[128,2,8,64]{3,0,2,1:T(8,128)} %get-tuple-element.14) | copy-start | bytes 1572868
  569.4 12.5 %copy-start.4 = (f32[128,2,8,64]{3,0,2,1:T(8,128)S(1)}, f32[128,2,8,64]{3,0,2,1:T(8,128)}, u32[]{:S(2)}) copy-start(f32[128,2,8,64]{3,0,2,1:T(8,128)} %copy-done.3) | copy-start | bytes 1572868
  616.0 13.3 %copy-start.87 = (bf16[2,2048,256]{2,1,0:T(8,128)(2,1)S(1)}, bf16[2,2048,256]{2,1,0:T(8,128)(2,1)}, u32[]{:S(2)}) copy-start(bf16[2,2048,256]{2,1,0:T(8,128)(2,1)} %param.27) | copy-start | bytes 6291460
  (77 other events, 356.0 us)
Sparse Core Ops, SparseCore 0:
  10.1 80.4 all-gather.4
  237.6 50.6 all-gather.6
  293.0 75.8 all-gather.8
  541.6 50.6 all-gather.10
where the time goes:
time: 680 us; the launch traced here: 674 us
  local copies, waits for them, and re-layouts  224 us (33%)
  matrix products  159 us (23%)
  waiting for transfers between devices  156 us (23%)
  other arithmetic  87.2 us (13%)
  blocking collectives  31.4 us (5%)
  between operations  15.9 us (2%)
    slice x60, local copies, waits for them, and re-layouts, solve_lower(): a_mat[..., row_at, col_at][..., None] * solved_rows[col_at]  95.2 us
    all_gather x1, waiting for transfers between devices, local(): gathered = lax.all_gather(mixed_out, 'tp', axis=1, tiled=True)  58.1 us
    dot_general x12, matrix products, project(): jnp.dot(portion, weight, preferred_element_type=jnp.float32)  55.6 us
    all_gather x2, waiting for transfers between devices, out_project(): lax.all_gather(blended_token_vectors, 'tp', axis=1, tiled=True)  50.8 us
    all_gather x1, waiting for transfers between devices, local(): lax.all_gather(residual_channel.reshape(row_count, own_width), 'tp', axis...  46 us
    unnamed x199, local copies, waits for them, and re-layouts  38.2 us
    dot_general x2, matrix products, delta_block(): jnp.einsum('bhsk,bhsv->bhkv', key_rows * jnp.exp(final_log - cumulative)[...  37 us
    psum x1, blocking collectives, post_residual(): squares = lax.psum(squares, 'tp')  31.4 us
  transfers between devices with their start and end apart: 4, of which 3 were waited for; matrix products, arithmetic and copies ran while one was open for 21% of the time, Pallas kernels for 0%

commit v1 on v0

v1 whole, which is shorter than its diff:
```python
import functools

import jax
import jax.numpy as jnp
from jax import lax
from jax.experimental import pallas as pl
from jax.experimental.pallas import tpu as pltpu
from jax.sharding import PartitionSpec as P

HEAD_DIM = 64
EPS = 1e-06
CHUNKS = 2
V_BLOCK = 16
VMEM_LIMIT = 60 * 1024 * 1024


def silu(value):
    return value * jax.nn.sigmoid(value)


def mix_kernel(*refs, steps, heads, seqs, with_residual, row_block):
    refs = list(refs)
    x_ref = refs.pop(0)
    if with_residual:
        m_ref = refs.pop(0)
        post_ref = refs.pop(0)
    (gain_ref, wq_ref, wk_ref, wv_ref, wg_ref, wab_ref, mag_ref, off_ref, sur_ref, read_ref, s_ref) = refs[:11]
    refs = refs[11:]
    y_ref = refs.pop(0)
    s_out = refs.pop(0)
    if with_residual:
        rms_out = refs.pop(0)
    (q_p, k_p, v_p, g_p, ab_p, q_t, k_t, v_t, kd_t, o_t) = refs
    parts, rows, width = x_ref.shape
    total = parts * width
    mix = wq_ref.shape[1]
    lanes = heads * seqs
    step = pl.program_id(0)

    if with_residual:
        squares = jnp.zeros((rows, width), jnp.float32)
        for part in range(parts):
            piece = m_ref[part].astype(jnp.float32)
            squares = squares + piece * piece
        post = lax.rsqrt(jnp.sum(squares, axis=1, keepdims=True) / total + EPS)
        rms_out[...] = post
    pieces = []
    squares = jnp.zeros((rows, width), jnp.float32)
    for part in range(parts):
        piece = x_ref[part].astype(jnp.float32)
        if with_residual:
            moved = m_ref[part].astype(jnp.float32) * post * post_ref[part]
            rounded = (piece + moved).astype(jnp.bfloat16)
            pieces.append(rounded)
            piece = rounded.astype(jnp.float32)
        squares = squares + piece * piece
    inv = lax.rsqrt(jnp.sum(squares, axis=1, keepdims=True) / total + EPS)
    hidden = []
    for part in range(parts):
        piece = pieces[part] if with_residual else x_ref[part]
        hidden.append((piece.astype(jnp.float32) * inv * gain_ref[part]).astype(jnp.bfloat16))
    hidden = jnp.concatenate(hidden, axis=1) if parts > 1 else hidden[0]

    def dot(weight):
        return (
            jnp.dot(hidden, weight, preferred_element_type=jnp.float32)
            .astype(jnp.bfloat16)
            .astype(jnp.float32)
        )

    at = pl.ds(pl.multiple_of(step * row_block, row_block), row_block)
    if mix % 128 == 0:
        qk = dot(jnp.concatenate([wq_ref[...], wk_ref[...]], axis=1))
        q_p[at, :] = qk[:, :mix]
        k_p[at, :] = qk[:, mix:]
        vg = dot(jnp.concatenate([wv_ref[...], wg_ref[...]], axis=1))
        v_p[at, :] = vg[:, :mix]
        g_p[at, :] = vg[:, mix:]
    else:
        q_p[at, :] = dot(wq_ref[...])
        k_p[at, :] = dot(wk_ref[...])
        v_p[at, :] = dot(wv_ref[...])
        g_p[at, :] = dot(wg_ref[...])
    ab_p[at, :] = dot(wab_ref[...])

    @pl.when(step == pl.num_programs(0) - 1)
    def _():
        def heads_to_lanes(ref, t, height):
            flipped = ref[pl.ds(t, seqs, stride=steps), :].T
            if heads == 1:
                return flipped[:height]
            return jnp.concatenate(
                [flipped[h * height : (h + 1) * height] for h in range(heads)], axis=1
            )

        cumulative = []
        strength = []
        for t in range(steps):
            pre = ab_p[pl.ds(t, seqs, stride=steps), :].T
            decay = [pre[h : h + 1] for h in range(heads)]
            write = [pre[heads + h : heads + h + 1] for h in range(heads)]
            decay = jnp.concatenate(decay, axis=1) if heads > 1 else decay[0]
            write = jnp.concatenate(write, axis=1) if heads > 1 else write[0]
            shifted = decay + off_ref[...]
            softplus = jnp.maximum(shifted, 0.0) + jnp.log1p(jnp.exp(-jnp.abs(shifted)))
            log_alpha = -jnp.exp(mag_ref[...]) * softplus + sur_ref[t : t + 1, :]
            cumulative.append(log_alpha if t == 0 else cumulative[-1] + log_alpha)
            strength.append(jax.nn.sigmoid(write))
        last = cumulative[-1]
        grown = [jnp.exp(value) for value in cumulative]

        for t in range(steps):
            span = pl.ds(t * HEAD_DIM, HEAD_DIM)
            query = silu(heads_to_lanes(q_p, t, HEAD_DIM))
            query = query * lax.rsqrt(jnp.sum(query * query, axis=0, keepdims=True) + EPS)
            q_t[span, :] = query * HEAD_DIM ** (-0.5)
            key = silu(heads_to_lanes(k_p, t, HEAD_DIM))
            key = key * lax.rsqrt(jnp.sum(key * key, axis=0, keepdims=True) + EPS)
            k_t[span, :] = key
            kd_t[span, :] = key * jnp.exp(last - cumulative[t])
            v_t[span, :] = silu(heads_to_lanes(v_p, t, HEAD_DIM)) * strength[t]

        a_mat = {}
        score = {}
        for t in range(steps):
            span = pl.ds(t * HEAD_DIM, HEAD_DIM)
            for s in range(t + 1):
                other = k_t[pl.ds(s * HEAD_DIM, HEAD_DIM), :]
                decay = jnp.exp(cumulative[t] - cumulative[s])
                score[t, s] = jnp.sum(q_t[span, :] * other, axis=0, keepdims=True) * decay
                if s < t:
                    gram = jnp.sum(k_t[span, :] * other, axis=0, keepdims=True)
                    a_mat[t, s] = gram * decay * strength[t]
        grown_strength = [grown[t] * strength[t] for t in range(steps)]

        def body(at_block, carry):
            base = pl.multiple_of(at_block * V_BLOCK, V_BLOCK)
            from_k = [jnp.zeros((V_BLOCK, lanes), jnp.float32) for _ in range(steps)]
            from_q = [jnp.zeros((V_BLOCK, lanes), jnp.float32) for _ in range(steps)]
            for d in range(HEAD_DIM):
                state = s_ref[pl.ds(base + d * HEAD_DIM, V_BLOCK), :]
                for t in range(steps):
                    from_k[t] = from_k[t] + k_t[pl.ds(t * HEAD_DIM + d, 1), :] * state
                    from_q[t] = from_q[t] + q_t[pl.ds(t * HEAD_DIM + d, 1), :] * state
            update = []
            for t in range(steps):
                current = v_t[pl.ds(base + t * HEAD_DIM, V_BLOCK), :] - grown_strength[t] * from_k[t]
                for s in range(t):
                    current = current - a_mat[t, s] * update[s]
                update.append(current)
                output = grown[t] * from_q[t]
                for s in range(t + 1):
                    output = output + score[t, s] * update[s]
                o_t[pl.ds(base + t * HEAD_DIM, V_BLOCK), :] = output
            final = grown[-1]
            for d in range(HEAD_DIM):
                state = s_ref[pl.ds(base + d * HEAD_DIM, V_BLOCK), :] * final
                for t in range(steps):
                    state = state + kd_t[pl.ds(t * HEAD_DIM + d, 1), :] * update[t]
                s_out[pl.ds(base + d * HEAD_DIM, V_BLOCK), :] = state
            return carry

        lax.fori_loop(0, HEAD_DIM // V_BLOCK, body, 0)

        for t in range(steps):
            output = o_t[pl.ds(t * HEAD_DIM, HEAD_DIM), :]
            square = jnp.sum(output * output, axis=0, keepdims=True) / HEAD_DIM
            normed = output * lax.rsqrt(square + EPS) * read_ref[...]
            normed = normed * silu(heads_to_lanes(g_p, t, HEAD_DIM))
            if heads > 1:
                normed = jnp.concatenate(
                    [normed[:, h * seqs : (h + 1) * seqs] for h in range(heads)], axis=0
                )
            q_p[pl.ds(t, seqs, stride=steps), :] = normed.T
        y_ref[...] = q_p[...].astype(jnp.bfloat16)


def whole_block(array):
    return pl.BlockSpec(array.shape, lambda i: (0,) * array.ndim)


def mix_call(x, m, post, gain, weights, small, state, steps, heads, seqs):
    parts, rows, width = x.shape
    row_block = rows // 4
    lanes = heads * seqs
    mix = weights[0].shape[1]
    stack = pl.BlockSpec((parts, row_block, width), lambda i: (0, i, 0))
    operands = [x]
    in_specs = [stack]
    if m is not None:
        operands += [m, post]
        in_specs += [stack, whole_block(post)]
    tail = [gain, *weights, *small, state]
    operands += tail
    in_specs += [whole_block(array) for array in tail]
    out_shape = [
        jax.ShapeDtypeStruct((rows, mix), jnp.bfloat16),
        jax.ShapeDtypeStruct(state.shape, jnp.float32),
    ]
    out_specs = [
        pl.BlockSpec((rows, mix), lambda i: (0, 0)),
        pl.BlockSpec(state.shape, lambda i: (0, 0)),
    ]
    if m is not None:
        out_shape.append(jax.ShapeDtypeStruct((rows, 1), jnp.float32))
        out_specs.append(pl.BlockSpec((row_block, 1), lambda i: (i, 0)))
    proj = pltpu.VMEM((rows, mix), jnp.float32)
    turned = pltpu.VMEM((steps * HEAD_DIM, lanes), jnp.float32)
    return pl.pallas_call(
        functools.partial(
            mix_kernel,
            steps=steps,
            heads=heads,
            seqs=seqs,
            with_residual=m is not None,
            row_block=row_block,
        ),
        grid=(4,),
        in_specs=in_specs,
        out_specs=out_specs,
        out_shape=out_shape,
        scratch_shapes=[proj] * 4
        + [pltpu.VMEM((rows, weights[4].shape[1]), jnp.float32)]
        + [turned] * 5,
        compiler_params=pltpu.CompilerParams(
            dimension_semantics=("arbitrary",), vmem_limit_bytes=VMEM_LIMIT
        ),
        cost_estimate=pl.CostEstimate(
            flops=20_000_000_000, transcendentals=0, bytes_accessed=14_000_000
        ),
        name="mix",
    )(*operands)


def out_kernel(y_ref, w_ref, m_ref, sq_ref):
    parts, rows, width = y_ref.shape
    joined = jnp.concatenate([y_ref[part] for part in range(parts)], axis=1)
    total = jnp.dot(joined, w_ref[...], preferred_element_type=jnp.float32)
    rounded = total.astype(jnp.bfloat16)
    m_ref[...] = rounded
    wide = rounded.astype(jnp.float32)
    sq_ref[...] = jnp.sum(wide * wide, axis=1, keepdims=True)


def out_call(y, weight):
    parts, rows, width = y.shape
    return pl.pallas_call(
        out_kernel,
        grid=(2,),
        in_specs=[
            pl.BlockSpec((parts, rows // 2, width), lambda i: (0, i, 0)),
            whole_block(weight),
        ],
        out_specs=[
            pl.BlockSpec((rows // 2, weight.shape[1]), lambda i: (i, 0)),
            pl.BlockSpec((rows // 2, 1), lambda i: (i, 0)),
        ],
        out_shape=[
            jax.ShapeDtypeStruct((rows, weight.shape[1]), jnp.bfloat16),
            jax.ShapeDtypeStruct((rows, 1), jnp.float32),
        ],
        compiler_params=pltpu.CompilerParams(
            dimension_semantics=("arbitrary",), vmem_limit_bytes=VMEM_LIMIT
        ),
        cost_estimate=pl.CostEstimate(
            flops=4_000_000_000, transcendentals=0, bytes_accessed=4_000_000
        ),
        name="out_proj",
    )(y, weight)


def local(
    residual_channel,
    prior_block_multiplier,
    probe_map_matrix,
    lookup_map_matrix,
    content_map_matrix,
    emission_valve_matrix,
    forgetting_map_matrix,
    insertion_rate_matrix,
    forgetting_magnitude_exponent,
    channel_forgetting_offset,
    surplus_forgetting_amounts,
    readout_rescale_multiplier,
    emission_map_matrix,
    post_mixing_multiplier,
    recurrent_matrices,
):
    layers = recurrent_matrices.shape[0]
    batch, steps, own = residual_channel.shape
    heads = recurrent_matrices.shape[2]
    cells = recurrent_matrices.shape[3]
    seqs = batch // CHUNKS
    rows = seqs * steps
    lanes = heads * seqs
    tp = lax.axis_size("tp")
    total = tp * own
    head_at = lax.axis_index("tp") * heads
    col_at = lax.axis_index("tp") * own

    state_in = recurrent_matrices.reshape(layers, CHUNKS, seqs, heads, cells)
    state_in = state_in.transpose(0, 1, 4, 3, 2).reshape(layers, CHUNKS, cells, lanes)
    surplus = surplus_forgetting_amounts.reshape(layers, CHUNKS, seqs, steps, heads)
    surplus = surplus.transpose(0, 1, 3, 4, 2).reshape(layers, CHUNKS, steps, lanes)

    def slice_heads(array, layer):
        return lax.dynamic_slice_in_dim(array[layer], head_at, heads, 1)

    shared = []
    for layer in range(layers):
        pair = jnp.concatenate(
            [slice_heads(forgetting_map_matrix, layer), slice_heads(insertion_rate_matrix, layer)],
            axis=1,
        )
        pair = jnp.pad(pair, ((0, 0), (0, 128 - 2 * heads)))
        weights = (
            probe_map_matrix[layer],
            lookup_map_matrix[layer],
            content_map_matrix[layer],
            emission_valve_matrix[layer],
            pair,
        )
        mag = jnp.repeat(forgetting_magnitude_exponent[layer], seqs)[None]
        off = jnp.repeat(channel_forgetting_offset[layer], seqs)[None]
        read = readout_rescale_multiplier[layer].reshape(heads, HEAD_DIM).T
        read = jnp.broadcast_to(read[:, :, None], (HEAD_DIM, heads, seqs)).reshape(HEAD_DIM, lanes)
        gain = prior_block_multiplier[layer].reshape(tp, 1, own)
        shared.append((weights, mag, off, read, gain))
    post_gain = post_mixing_multiplier.reshape(layers, tp, 1, own)
    own_gain = lax.dynamic_slice_in_dim(post_mixing_multiplier, col_at, own, 1)

    x_own = [
        residual_channel[c * seqs : (c + 1) * seqs].reshape(rows, own) for c in range(CHUNKS)
    ]
    x_all = [lax.all_gather(x_own[c], "tp", axis=0) for c in range(CHUNKS)]
    mixed_all = [None] * CHUNKS
    states = [[None] * CHUNKS for _ in range(layers)]
    squares = [None] * CHUNKS
    mixed = [None] * CHUNKS
    for layer in range(layers):
        weights, mag, off, read, gain = shared[layer]
        for c in range(CHUNKS):
            previous = None if layer == 0 else post_gain[layer - 1]
            result = mix_call(
                x_all[c],
                mixed_all[c],
                previous,
                gain,
                weights,
                (mag, off, surplus[layer, c], read),
                state_in[layer, c],
                steps,
                heads,
                seqs,
            )
            states[layer][c] = result[1]
            if layer > 0:
                moved = mixed[c].astype(jnp.float32) * result[2] * own_gain[layer - 1]
                x_own[c] = (x_own[c].astype(jnp.float32) + moved).astype(jnp.bfloat16)
            y_all = lax.all_gather(result[0], "tp", axis=0)
            mixed[c], squares[c] = out_call(y_all, emission_map_matrix[layer])
            if layer < layers - 1:
                mixed_all[c] = lax.all_gather(mixed[c], "tp", axis=0)
    joined = lax.psum(jnp.concatenate([s[:, 0] for s in squares]), "tp")
    post = lax.rsqrt(joined / total + EPS)[:, None]
    stream = jnp.concatenate(x_own, axis=0).astype(jnp.float32)
    moved = jnp.concatenate(mixed, axis=0).astype(jnp.float32)
    new_stream = (stream + moved * post * own_gain[layers - 1]).astype(jnp.bfloat16)
    memory = jnp.stack([jnp.stack(states[layer]) for layer in range(layers)])
    memory = memory.reshape(layers, CHUNKS, cells, heads, seqs).transpose(0, 1, 4, 3, 2)
    return (
        new_stream.reshape(batch, steps, own),
        memory.reshape(layers, batch, heads, cells),
    )


def solution(mesh):
    return jax.shard_map(
        local,
        mesh=mesh,
        in_specs=(
            P("grp", None, "tp"),
            P(),
            P(None, None, "tp"),
            P(None, None, "tp"),
            P(None, None, "tp"),
            P(None, None, "tp"),
            P(),
            P(),
            P(None, "tp"),
            P(None, "tp"),
            P(None, "grp", None, "tp"),
            P(None, "tp"),
            P(None, None, "tp"),
            P(),
            P(None, "grp", "tp", None),
        ),
        out_specs=(P("grp", None, "tp"), P(None, "grp", "tp", None)),
        check_vma=False,
    )
```

time: 680 us -> 432 us (0.64)
  matrix products: 159 us -> 0 us
  local copies, waits for them, and re-layouts: 224 us -> 67 us
  Pallas kernels: 0 us -> 87.2 us
  other arithmetic: 87.2 us -> 8.08 us
  waiting for transfers between devices: 156 us -> 223 us
    dot_general x26 -> x0, matrix products: 159 us -> none  [the longest x12 55.6 us: project(): jnp.dot(portion, weight, preferred_element_type=jnp.float32)]
    slice x69 -> x7, local copies, waits for them, and re-layouts: 115 us -> 5.37 us  [the longest x1 2.92 us: local(): state_in[layer, c]]
    pallas_call x0 -> x8, Pallas kernels: none -> 87.2 us  [the longest x4 74.2 us: mix_call(): pl.pallas_call(functools.partial(mix_kernel, steps=steps, heads=heads, se...]
    all_gather x4 -> x8, waiting for transfers between devices: 155 us -> 222 us  [the longest x4 95.5 us: local(): y_all = lax.all_gather(result[0], 'tp', axis=0)]
    convert_element_type x7 -> x2, other arithmetic: 44.5 us -> 2.35 us  [the longest x1 2.04 us: local(): (stream + moved * post * own_gain[layers - 1]).astype(jnp.bfloat16)]
    add x2 -> x0, local copies, waits for them, and re-layouts: 16.1 us -> none  [delta_block(): jnp.exp(final_log)[..., None] * matrix_state]
    reduce_sum x8 -> x0, other arithmetic: 14.3 us -> none  [the longest x2 6.76 us: local(): jnp.mean(widened * widened, axis=-1, keepdims=True) + EPS]
    another operation x4 -> x7, local copies, waits for them, and re-layouts: 18.6 us -> 4.52 us  [the longest x1 1.91 us: local(): x_all = [lax.all_gather(x_own[c], 'tp', axis=0) for c in range(CHUNKS)]]
  transfers between devices with their start and end apart: 4 -> 8, of which waited for: 3 -> 7; matrix products, arithmetic and copies ran while one was open for 21% -> 16% of each run, Pallas kernels for 0% -> 19%
where the time goes in v1:
time: 432 us; the launch traced here: 431 us
  waiting for transfers between devices  223 us (52%)
  Pallas kernels  87.2 us (20%)
  local copies, waits for them, and re-layouts  67 us (16%)
  blocking collectives  31.4 us (7%)
  between operations  14.4 us (3%)
  other arithmetic  8.08 us (2%)
    all_gather x4, waiting for transfers between devices, local(): y_all = lax.all_gather(result[0], 'tp', axis=0)  95.5 us
    pallas_call x4, Pallas kernels, mix_call(): pl.pallas_call(functools.partial(mix_kernel, steps=steps, heads=heads, se...  74.2 us
    all_gather x2, waiting for transfers between devices, local(): mixed_all[c] = lax.all_gather(mixed[c], 'tp', axis=0)  70 us
    all_gather x2, waiting for transfers between devices, local(): x_all = [lax.all_gather(x_own[c], 'tp', axis=0) for c in range(CHUNKS)]  56.7 us
    psum x1, blocking collectives, local(): joined = lax.psum(jnp.concatenate([s[:, 0] for s in squares]), 'tp')  31.4 us
    unnamed x38, local copies, waits for them, and re-layouts  28.9 us
    pallas_call x4, Pallas kernels, out_call(): pl.pallas_call(out_kernel, grid=(2,), in_specs=[pl.BlockSpec((parts, rows...  13 us
    pallas_call x4, local copies, waits for them, and re-layouts, mix_call(): pl.pallas_call(functools.partial(mix_kernel, steps=steps, heads=heads, se...  10.8 us
  transfers between devices with their start and end apart: 8, of which 7 were waited for; matrix products, arithmetic and copies ran while one was open for 16% of the time, Pallas kernels for 19%

profile of v1, /device:TPU:0, one launch (start us, length us, event | category | flops | bytes accessed | tf_op | source)
XLA Modules:
  0.0 431.4 jit_solution(5175596817208493729)
XLA Ops:
  11.8 8.3 %copy.63 = f32[2,128,2,4096]{3,1,2,0:T(8,128)S(1)} copy(f32[2,128,2,4096]{3,2,1,0:T(2,128)} %param.29) | data formatting | bytes 16777216 | tf_op args[14]
  21.0 2.9 fusion.5
  24.0 3.1 copy.79
  32.2 3.8 slice_bitcast_fusion.1
  38.0 25.3 %all-gather.17.cloned.1.call-done.refs_0_ = bf16[16,512,256]{2,1,0:T(8,128)(2,1)} async-done(((bf16[1,512,256]{2,1,0:T(8,128)(2,1)}), bf16[16,512,256]{2,1,0:T(8,128)(2,1)}) %all-gather.17.cloned.1.call-update) | async-done | bytes 4194320 | tf_op jit(solution)/shard_map/all_gather | solution.py:335
  63.3 17.3 %mix.6 = (bf16[512,128]{1,0:T(8,128)(2,1)}, f32[4096,128]{1,0:T(8,128)}) custom-call(bf16[16,512,256]{2,1,0:T(8,128)(2,1)} %all-gather.17.cloned.1.call-done.refs_0_, f32[16,1,256]{2,1,0:T(1,128)} %bitcast.113, bf16[4096,128]{1,0:T(8,128)(2,1)} %get-tuple-element.80.refs_2_, bf16[4096,128]{1,0:T(8,128)(2,1)} %get-tuple-element.51.refs_3_, ...), custom_call_target="tpu_custom_call" | custom-call | flops 20000000000 | bytes 14000000 | tf_op jit(solution)/shard_map/mix/pallas_call | solution.py:209
  83.5 31.4 %all-gather.15.cloned.1.call-done.refs_0_ = bf16[16,512,256]{2,1,0:T(8,128)(2,1)} async-done(((bf16[1,512,256]{2,1,0:T(8,128)(2,1)}), bf16[16,512,256]{2,1,0:T(8,128)(2,1)}) %all-gather.15.cloned.1.call-update) | async-done | bytes 4194320 | tf_op jit(solution)/shard_map/all_gather | solution.py:335
  115.0 17.3 %mix.4 = (bf16[512,128]{1,0:T(8,128)(2,1)}, f32[4096,128]{1,0:T(8,128)}) custom-call(bf16[16,512,256]{2,1,0:T(8,128)(2,1)} %all-gather.15.cloned.1.call-done.refs_0_, f32[16,1,256]{2,1,0:T(1,128)} %bitcast.114, bf16[4096,128]{1,0:T(8,128)(2,1)} %get-tuple-element.80.refs_2_, bf16[4096,128]{1,0:T(8,128)(2,1)} %get-tuple-element.51.refs_3_, ...), custom_call_target="tpu_custom_call" | custom-call | flops 20000000000 | bytes 14000000 | tf_op jit(solution)/shard_map/mix/pallas_call | solution.py:209
  132.3 3.0 slice_bitcast_fusion
  135.3 21.9 %all-gather.23.cloned.1.call-done = bf16[8192,128]{1,0:T(8,128)(2,1)} async-done(((bf16[512,128]{1,0:T(8,128)(2,1)}), bf16[8192,128]{1,0:T(8,128)(2,1)}) %all-gather.23.cloned.1.call-update) | async-done | bytes 2097168 | tf_op jit(solution)/shard_map/all_gather | solution.py:360
  157.2 3.2 out_proj.5
  160.5 38.9 %all-gather.19.cloned.1.call-done = bf16[8192,128]{1,0:T(8,128)(2,1)} async-done(((bf16[512,128]{1,0:T(8,128)(2,1)}), bf16[8192,128]{1,0:T(8,128)(2,1)}) %all-gather.19.cloned.1.call-update) | async-done | bytes 2097168 | tf_op jit(solution)/shard_map/all_gather | solution.py:360
  199.5 3.2 out_proj.4
  210.4 40.2 %all-gather.25.cloned.1.call-done = bf16[8192,256]{1,0:T(8,128)(2,1)} async-done(((bf16[512,256]{1,0:T(8,128)(2,1)}), bf16[8192,256]{1,0:T(8,128)(2,1)}) %all-gather.25.cloned.1.call-update) | async-done | bytes 4194320 | tf_op jit(solution)/shard_map/all_gather | solution.py:363
  250.6 19.8 %mix.7 = (bf16[512,128]{1,0:T(8,128)(2,1)}, f32[4096,128]{1,0:T(8,128)}, f32[512,1]{1,0:T(8,128)}) custom-call(bf16[16,512,256]{2,1,0:T(8,128)(2,1)} %all-gather.17.cloned.1.call-done.refs_0_, bf16[16,512,256]{2,1,0:T(8,128)(2,1)} %bitcast.120, f32[16,1,256]{2,1,0:T(1,128)} %bitcast.109, f32[16,1,256]{2,1,0:T(1,128)} %bitcast.111, ...), custom_call_target="tpu_custom_call" | custom-call | flops 20000000000 | bytes 14000000 | tf_op jit(solution)/shard_map/mix/pallas_call | solution.py:209
  272.3 29.8 %all-gather.21.cloned.1.call-done = bf16[8192,256]{1,0:T(8,128)(2,1)} async-done(((bf16[512,256]{1,0:T(8,128)(2,1)}), bf16[8192,256]{1,0:T(8,128)(2,1)}) %all-gather.21.cloned.1.call-update) | async-done | bytes 4194320 | tf_op jit(solution)/shard_map/all_gather | solution.py:363
  302.1 19.8 %mix.5 = (bf16[512,128]{1,0:T(8,128)(2,1)}, f32[4096,128]{1,0:T(8,128)}, f32[512,1]{1,0:T(8,128)}) custom-call(bf16[16,512,256]{2,1,0:T(8,128)(2,1)} %all-gather.15.cloned.1.call-done.refs_0_, bf16[16,512,256]{2,1,0:T(8,128)(2,1)} %bitcast.119, f32[16,1,256]{2,1,0:T(1,128)} %bitcast.110, f32[16,1,256]{2,1,0:T(1,128)} %bitcast.112, ...), custom_call_target="tpu_custom_call" | custom-call | flops 20000000000 | bytes 14000000 | tf_op jit(solution)/shard_map/mix/pallas_call | solution.py:209
  326.9 3.1 copy.74
  332.9 3.2 maximum_bitcast_fusion
  337.1 9.9 %copy.76 = f32[2,128,2,4096]{3,2,1,0:T(2,128)} copy(f32[2,128,2,4096]{3,1,2,0:T(8,128)S(1)} %bitcast.98) | data formatting | bytes 16777216
  347.7 3.3 out_proj.7
  352.0 34.7 %all-gather.27.cloned.1.call-done = bf16[8192,128]{1,0:T(8,128)(2,1)} async-done(((bf16[512,128]{1,0:T(8,128)(2,1)}), bf16[8192,128]{1,0:T(8,128)(2,1)}) %all-gather.27.cloned.1.call-update) | async-done | bytes 2097168 | tf_op jit(solution)/shard_map/all_gather | solution.py:360
  386.7 3.3 out_proj.6
  391.0 31.4 %psum.7 = f32[1024]{0:T(1024)S(1)} all-reduce(f32[1024]{0:T(1024)S(1)} %pad_maximum_fusion.2), channel_id=1, replica_groups=mesh['grp'=2,'tp'=16] {'tp'}, use_global_device_ids=true, to_apply=%region_0.1 | all-reduce | flops 1024 | bytes 8192 | tf_op jit(solution)/shard_map/psum | solution.py:364
  (104 shorter events, 39.0 us)
Async XLA Ops:
  7.2 3.9 copy-start.6
  7.2 56.1 %all-gather.17.cloned.1.call-start = ((), (), s32[]{:S(2)}) async-start(), calls=%async_computation.1 | async-start | bytes 4456448 | tf_op jit(solution)/shard_map/all_gather | solution.py:335
  9.1 105.8 %all-gather.15.cloned.1.call-start = ((), (), s32[]{:S(2)}) async-start(), calls=%async_computation | async-start | bytes 4456448 | tf_op jit(solution)/shard_map/all_gather | solution.py:335
  9.9 147.3 %all-gather.23.cloned.1.call-start = ((), (), s32[]{:S(2)}) async-start(), calls=%async_computation.4 | async-start | bytes 2228224 | tf_op jit(solution)/shard_map/all_gather | solution.py:360
  24.0 3.1 copy-start.11
  24.0 3.3 copy-start.13
  24.0 4.4 %copy-start.14 = (f32[2,2]{1,0:T(2,128)S(1)}, f32[2,2]{1,0:T(2,128)}, u32[]{:S(2)}) copy-start(f32[2,2]{1,0:T(2,128)} %param.23) | copy-start | bytes 52
  24.0 5.1 %copy-start.15 = (f32[2,2]{1,0:T(2,128)S(1)}, f32[2,2]{1,0:T(2,128)}, u32[]{:S(2)}) copy-start(f32[2,2]{1,0:T(2,128)} %param.24) | copy-start | bytes 52
  27.1 4.5 %copy-start.10 = (f32[2,4096]{1,0:T(2,128)S(1)}, f32[2,4096]{1,0:T(2,128)}, u32[]{:S(2)}) copy-start(f32[2,4096]{1,0:T(2,128)} %param.16) | copy-start | bytes 98308
  29.7 2.4 copy-start.1
  32.2 3.8 copy-start.2
  32.2 3.8 copy-start.3
  80.6 118.8 %all-gather.19.cloned.1.call-start = ((), (), s32[]{:S(2)}) async-start(), calls=%async_computation.2 | async-start | bytes 2228224 | tf_op jit(solution)/shard_map/all_gather | solution.py:360
  132.3 118.3 %all-gather.25.cloned.1.call-start = ((), (), s32[]{:S(2)}) async-start(), calls=%async_computation.5 | async-start | bytes 4456448 | tf_op jit(solution)/shard_map/all_gather | solution.py:363
  160.5 141.6 %all-gather.21.cloned.1.call-start = ((), (), s32[]{:S(2)}) async-start(), calls=%async_computation.3 | async-start | bytes 4456448 | tf_op jit(solution)/shard_map/all_gather | solution.py:363
  202.7 144.9 %all-gather.29.cloned.1.call-start = ((), (), s32[]{:S(2)}) async-start(), calls=%async_computation.7 | async-start | bytes 2228224 | tf_op jit(solution)/shard_map/all_gather | solution.py:360
  204.5 5.3 %copy-start.12 = (f32[2,4096]{1,0:T(2,128)S(1)}, f32[2,4096]{1,0:T(2,128)}, u32[]{:S(2)}) copy-start(f32[2,4096]{1,0:T(2,128)} %param.28) | copy-start | bytes 98308
  270.4 116.3 %all-gather.27.cloned.1.call-start = ((), (), s32[]{:S(2)}) async-start(), calls=%async_computation.6 | async-start | bytes 2228224 | tf_op jit(solution)/shard_map/all_gather | solution.py:360
  337.1 9.9 %copy-start.7 = (f32[512,1]{1,0:T(8,128)S(1)}, f32[512,1]{1,0:T(8,128)}, u32[]{:S(2)}) copy-start(f32[512,1]{1,0:T(8,128)} %get-tuple-element.23) | copy-start | bytes 6148
  337.1 10.1 %copy-start.8 = (f32[512,1]{1,0:T(8,128)S(1)}, f32[512,1]{1,0:T(8,128)}, u32[]{:S(2)}) copy-start(f32[512,1]{1,0:T(8,128)} %get-tuple-element.20) | copy-start | bytes 6148
  337.1 10.2 %copy-start = (bf16[128,8,256]{2,1,0:T(8,128)(2,1)S(1)}, bf16[128,8,256]{2,1,0:T(8,128)(2,1)}, u32[]{:S(2)}) copy-start(bf16[128,8,256]{2,1,0:T(8,128)(2,1)} %param.15) | copy-start | bytes 1572868
  337.1 10.2 %copy-start.4 = (bf16[512,256]{1,0:T(8,128)(2,1)S(1)}, bf16[512,256]{1,0:T(8,128)(2,1)}, u32[]{:S(2)}) copy-start(bf16[512,256]{1,0:T(8,128)(2,1)} %get-tuple-element.22) | copy-start | bytes 786436
  337.1 10.2 %copy-start.5 = (bf16[512,256]{1,0:T(8,128)(2,1)S(1)}, bf16[512,256]{1,0:T(8,128)(2,1)}, u32[]{:S(2)}) copy-start(bf16[512,256]{1,0:T(8,128)(2,1)} %get-tuple-element.19) | copy-start | bytes 786436
  386.7 35.8 %copy-start.9 = (bf16[512,256]{1,0:T(8,128)(2,1)S(1)}, bf16[512,256]{1,0:T(8,128)(2,1)}, u32[]{:S(2)}) copy-start(bf16[512,256]{1,0:T(8,128)(2,1)} %get-tuple-element.27) | copy-start | bytes 786436
Sparse Core Ops, SparseCore 0:
  10.1 53.0 all-gather.16
  66.0 48.9 all-gather.14
  117.1 40.0 all-gather.22
  159.3 40.1 all-gather.18
  201.5 49.0 all-gather.24
  253.2 48.8 all-gather.20
  304.3 39.9 all-gather.28
  346.5 40.1 all-gather.26

commit v2 on v1

--- a/solution.py
+++ b/solution.py
@@ -11,6 +11,7 @@
 EPS = 1e-06
 CHUNKS = 2
 V_BLOCK = 16
+ROW_STEPS = 4
 VMEM_LIMIT = 60 * 1024 * 1024
 
 
@@ -35,7 +36,7 @@
     total = parts * width
     mix = wq_ref.shape[1]
     lanes = heads * seqs
-    step = pl.program_id(0)
+    step = pl.program_id(0) % ROW_STEPS
 
     if with_residual:
         squares = jnp.zeros((rows, width), jnp.float32)
@@ -83,7 +84,7 @@
         g_p[at, :] = dot(wg_ref[...])
     ab_p[at, :] = dot(wab_ref[...])
 
-    @pl.when(step == pl.num_programs(0) - 1)
+    @pl.when(step == ROW_STEPS - 1)
     def _():
         def heads_to_lanes(ref, t, height):
             flipped = ref[pl.ds(t, seqs, stride=steps), :].T
@@ -181,8 +182,9 @@
 
 def mix_call(x, m, post, gain, weights, small, state, steps, heads, seqs):
     parts, rows, width = x.shape
-    row_block = rows // 4
-    lanes = heads * seqs
+    chunks, cells, lanes = state.shape
+    chunk_rows = rows // chunks
+    row_block = chunk_rows // ROW_STEPS
     mix = weights[0].shape[1]
     stack = pl.BlockSpec((parts, row_block, width), lambda i: (0, i, 0))
     operands = [x]
@@ -190,21 +192,24 @@
     if m is not None:
         operands += [m, post]
         in_specs += [stack, whole_block(post)]
-    tail = [gain, *weights, *small, state]
-    operands += tail
+    mag, off, surplus, read = small
+    chunked = lambda *block: pl.BlockSpec((None, *block), lambda i: (i // ROW_STEPS, 0, 0))
+    tail = [gain, *weights, mag, off]
+    operands += [*tail, surplus, read, state]
     in_specs += [whole_block(array) for array in tail]
+    in_specs += [chunked(steps, lanes), whole_block(read), chunked(cells, lanes)]
     out_shape = [
         jax.ShapeDtypeStruct((rows, mix), jnp.bfloat16),
         jax.ShapeDtypeStruct(state.shape, jnp.float32),
     ]
     out_specs = [
-        pl.BlockSpec((rows, mix), lambda i: (0, 0)),
-        pl.BlockSpec(state.shape, lambda i: (0, 0)),
+        pl.BlockSpec((chunk_rows, mix), lambda i: (i // ROW_STEPS, 0)),
+        chunked(cells, lanes),
     ]
     if m is not None:
         out_shape.append(jax.ShapeDtypeStruct((rows, 1), jnp.float32))
         out_specs.append(pl.BlockSpec((row_block, 1), lambda i: (i, 0)))
-    proj = pltpu.VMEM((rows, mix), jnp.float32)
+    proj = pltpu.VMEM((chunk_rows, mix), jnp.float32)
     turned = pltpu.VMEM((steps * HEAD_DIM, lanes), jnp.float32)
     return pl.pallas_call(
         functools.partial(
@@ -215,12 +220,12 @@
             with_residual=m is not None,
             row_block=row_block,
         ),
-        grid=(4,),
+        grid=(chunks * ROW_STEPS,),
         in_specs=in_specs,
         out_specs=out_specs,
         out_shape=out_shape,
         scratch_shapes=[proj] * 4
-        + [pltpu.VMEM((rows, weights[4].shape[1]), jnp.float32)]
+        + [pltpu.VMEM((chunk_rows, weights[4].shape[1]), jnp.float32)]
         + [turned] * 5,
         compiler_params=pltpu.CompilerParams(
             dimension_semantics=("arbitrary",), vmem_limit_bytes=VMEM_LIMIT
@@ -246,14 +251,14 @@
     parts, rows, width = y.shape
     return pl.pallas_call(
         out_kernel,
-        grid=(2,),
+        grid=(4,),
         in_specs=[
-            pl.BlockSpec((parts, rows // 2, width), lambda i: (0, i, 0)),
+            pl.BlockSpec((parts, rows // 4, width), lambda i: (0, i, 0)),
             whole_block(weight),
         ],
         out_specs=[
-            pl.BlockSpec((rows // 2, weight.shape[1]), lambda i: (i, 0)),
-            pl.BlockSpec((rows // 2, 1), lambda i: (i, 0)),
+            pl.BlockSpec((rows // 4, weight.shape[1]), lambda i: (i, 0)),
+            pl.BlockSpec((rows // 4, 1), lambda i: (i, 0)),
         ],
         out_shape=[
             jax.ShapeDtypeStruct((rows, weight.shape[1]), jnp.bfloat16),
@@ -267,6 +272,16 @@
         ),
         name="out_proj",
     )(y, weight)
+
+
+def sum_over_tp(values, size):
+    if size & (size - 1):
+        return lax.psum(values, "tp")
+    hop = 1
+    while hop < size:
+        values = values + lax.ppermute(values, "tp", [(i, i ^ hop) for i in range(size)])
+        hop *= 2
+    return values
 
 
 def local(
@@ -329,44 +344,37 @@
     post_gain = post_mixing_multiplier.reshape(layers, tp, 1, own)
     own_gain = lax.dynamic_slice_in_dim(post_mixing_multiplier, col_at, own, 1)
 
-    x_own = [
-        residual_channel[c * seqs : (c + 1) * seqs].reshape(rows, own) for c in range(CHUNKS)
-    ]
-    x_all = [lax.all_gather(x_own[c], "tp", axis=0) for c in range(CHUNKS)]
-    mixed_all = [None] * CHUNKS
-    states = [[None] * CHUNKS for _ in range(layers)]
-    squares = [None] * CHUNKS
-    mixed = [None] * CHUNKS
+    x_own = residual_channel.reshape(batch * steps, own)
+    x_all = lax.all_gather(x_own, "tp", axis=0)
+    stream = x_own.astype(jnp.float32)
+    mixed_all = None
+    states = []
     for layer in range(layers):
         weights, mag, off, read, gain = shared[layer]
-        for c in range(CHUNKS):
-            previous = None if layer == 0 else post_gain[layer - 1]
-            result = mix_call(
-                x_all[c],
-                mixed_all[c],
-                previous,
-                gain,
-                weights,
-                (mag, off, surplus[layer, c], read),
-                state_in[layer, c],
-                steps,
-                heads,
-                seqs,
-            )
-            states[layer][c] = result[1]
-            if layer > 0:
-                moved = mixed[c].astype(jnp.float32) * result[2] * own_gain[layer - 1]
-                x_own[c] = (x_own[c].astype(jnp.float32) + moved).astype(jnp.bfloat16)
-            y_all = lax.all_gather(result[0], "tp", axis=0)
-            mixed[c], squares[c] = out_call(y_all, emission_map_matrix[layer])
-            if layer < layers - 1:
-                mixed_all[c] = lax.all_gather(mixed[c], "tp", axis=0)
-    joined = lax.psum(jnp.concatenate([s[:, 0] for s in squares]), "tp")
-    post = lax.rsqrt(joined / total + EPS)[:, None]
-    stream = jnp.concatenate(x_own, axis=0).astype(jnp.float32)
-    moved = jnp.concatenate(mixed, axis=0).astype(jnp.float32)
+        result = mix_call(
+            x_all,
+            mixed_all,
+            None if layer == 0 else post_gain[layer - 1],
+            gain,
+            weights,
+            (mag, off, surplus[layer], read),
+            state_in[layer],
+            steps,
+            heads,
+            seqs,
+        )
+        states.append(result[1])
+        if layer > 0:
+            moved = mixed.astype(jnp.float32) * result[2] * own_gain[layer - 1]
+            stream = (stream + moved).astype(jnp.bfloat16).astype(jnp.float32)
+        y_all = lax.all_gather(result[0], "tp", axis=0)
+        mixed, squares = out_call(y_all, emission_map_matrix[layer])
+        if layer < layers - 1:
+            mixed_all = lax.all_gather(mixed, "tp", axis=0)
+    post = lax.rsqrt(sum_over_tp(squares[:, 0], tp) / total + EPS)[:, None]
+    moved = mixed.astype(jnp.float32)
     new_stream = (stream + moved * post * own_gain[layers - 1]).astype(jnp.bfloat16)
-    memory = jnp.stack([jnp.stack(states[layer]) for layer in range(layers)])
+    memory = jnp.stack(states)
     memory = memory.reshape(layers, CHUNKS, cells, heads, seqs).transpose(0, 1, 4, 3, 2)
     return (
         new_stream.reshape(batch, steps, own),

time: 432 us -> 385 us (0.89)
  blocking collectives: 31.4 us -> 0 us
  waiting for transfers between devices: 223 us -> 205 us
  Pallas kernels: 87.2 us -> 76.1 us
  local copies, waits for them, and re-layouts: 67 us -> 75.4 us
    psum x1 -> x0, blocking collectives: 31.4 us -> none  [local(): joined = lax.psum(jnp.concatenate([s[:, 0] for s in squares]), 'tp')]
    all_gather x4 -> x2, waiting for transfers between devices: 127 us -> 103 us  [the longest x1 57.1 us: local(): mixed_all = lax.all_gather(mixed, 'tp', axis=0)]
    squeeze x2 -> x5, local copies, waits for them, and re-layouts: 3.61 us -> 14.5 us  [the longest x2 11.6 us: local(): state_in[layer]]
    unnamed x38 -> x30, local copies, waits for them, and re-layouts: 28.9 us -> 18.2 us
    pallas_call x4 -> x2, Pallas kernels: 74.2 us -> 65.8 us  [mix_call(): pl.pallas_call(functools.partial(mix_kernel, steps=steps, heads=heads, se...]
    slice x3 -> x6, local copies, waits for them, and re-layouts: 3.61 us -> 10.3 us  [the longest x3 9.65 us: local(): state_in[layer]]
    transpose x1, other arithmetic: 3.17 us -> 7.9 us  [local(): memory.reshape(layers, CHUNKS, cells, heads, seqs).transpose(0, 1, 4, 3, 2)]
    pallas_call x4 -> x2, Pallas kernels: 13 us -> 10.4 us  [out_call(): pl.pallas_call(out_kernel, grid=(4,), in_specs=[pl.BlockSpec((parts, rows...]
  transfers between devices with their start and end apart: 8 -> 8, of which waited for: 7 -> 6; matrix products, arithmetic and copies ran while one was open for 16% -> 22% of each run, Pallas kernels for 19% -> 0%
where the time goes in v2:
time: 385 us; the launch traced here: 384 us
  waiting for transfers between devices  205 us (53%)
  Pallas kernels  76.1 us (20%)
  local copies, waits for them, and re-layouts  75.4 us (20%)
  between operations  14 us (4%)
  other arithmetic  10.7 us (3%)
    all_gather x2, waiting for transfers between devices, local(): y_all = lax.all_gather(result[0], 'tp', axis=0)  96.6 us
    pallas_call x2, Pallas kernels, mix_call(): pl.pallas_call(functools.partial(mix_kernel, steps=steps, heads=heads, se...  65.8 us
    all_gather x1, waiting for transfers between devices, local(): mixed_all = lax.all_gather(mixed, 'tp', axis=0)  57.1 us
    all_gather x1, waiting for transfers between devices, local(): x_all = lax.all_gather(x_own, 'tp', axis=0)  46.1 us
    unnamed x30, local copies, waits for them, and re-layouts  18.2 us
    squeeze x2, local copies, waits for them, and re-layouts, local(): state_in[layer]  11.6 us
    pallas_call x2, local copies, waits for them, and re-layouts, mix_call(): pl.pallas_call(functools.partial(mix_kernel, steps=steps, heads=heads, se...  11.3 us
    pallas_call x2, Pallas kernels, out_call(): pl.pallas_call(out_kernel, grid=(4,), in_specs=[pl.BlockSpec((parts, rows...  10.4 us
  transfers between devices with their start and end apart: 8, of which 6 were waited for; matrix products, arithmetic and copies ran while one was open for 22% of the time, Pallas kernels for 0%

profile of v2, /device:TPU:0, one launch (start us, length us, event | category | flops | bytes accessed | tf_op | source)
XLA Modules:
  0.0 384.3 jit_solution(13280924107731074328)
XLA Ops:
  10.8 8.3 %copy.56 = f32[2,128,2,4096]{3,1,2,0:T(8,128)S(1)} copy(f32[2,128,2,4096]{3,2,1,0:T(2,128)} %param.29) | data formatting | bytes 16777216 | tf_op args[14]
  19.1 2.8 fusion.2
  21.8 2.2 copy.57
  24.1 6.0 %copy.58.refs_11_ = f32[2,4096,128]{2,1,0:T(8,128)} copy(f32[2,4096,128]{1,2,0:T(8,128)} %bitcast.69) | data formatting | bytes 8388608 | tf_op jit(solution)/shard_map/squeeze | solution.py:361
  35.2 3.8 slice_bitcast_fusion.1
  39.0 2.1 slice_bitcast_fusion.3
  41.1 46.1 %all-gather.8.cloned.1.call-done.refs_0_ = bf16[16,1024,256]{2,1,0:T(8,128)(2,1)} async-done(((bf16[1,1024,256]{2,1,0:T(8,128)(2,1)}), bf16[16,1024,256]{2,1,0:T(8,128)(2,1)}) %all-gather.8.cloned.1.call-update) | async-done | bytes 8388624 | tf_op jit(solution)/shard_map/all_gather | solution.py:348
  87.2 30.7 %mix.2 = (bf16[1024,128]{1,0:T(8,128)(2,1)}, f32[2,4096,128]{2,1,0:T(8,128)}) custom-call(bf16[16,1024,256]{2,1,0:T(8,128)(2,1)} %all-gather.8.cloned.1.call-done.refs_0_, f32[16,1,256]{2,1,0:T(1,128)} %bitcast.77, bf16[4096,128]{1,0:T(8,128)(2,1)} %get-tuple-element.56.refs_2_, bf16[4096,128]{1,0:T(8,128)(2,1)} %get-tuple-element.33.refs_3_, ...), custom_call_target="tpu_custom_call" | custom-call | flops 20000000000 | bytes 14000000 | tf_op jit(solution)/shard_map/mix/pallas_call | solution.py:214
  118.0 1.5 slice_bitcast_fusion
  119.5 47.5 %all-gather.10.cloned.1.call-done = bf16[16384,128]{1,0:T(8,128)(2,1)} async-done(((bf16[1024,128]{1,0:T(8,128)(2,1)}), bf16[16384,128]{1,0:T(8,128)(2,1)}) %all-gather.10.cloned.1.call-update) | async-done | bytes 4194320 | tf_op jit(solution)/shard_map/all_gather | solution.py:370
  167.0 5.2 %out_proj.2 = (bf16[1024,256]{1,0:T(8,128)(2,1)}, f32[1024,1]{1,0:T(8,128)}) custom-call(bf16[16,1024,128]{2,1,0:T(8,128)(2,1)} %bitcast.83, bf16[2048,256]{1,0:T(8,128)(2,1)} %get-tuple-element.27.w_ref), custom_call_target="tpu_custom_call" | custom-call | flops 4000000000 | bytes 4000000 | tf_op jit(solution)/shard_map/out_proj/pallas_call | solution.py:252
  174.0 4.7 %copy.61 = f32[1,2,4096,2,64]{2,4,3,1,0:T(8,128)} copy(f32[1,2,4096,2,64]{2,4,1,3,0:T(8,128)} %get-tuple-element.24) | data formatting | bytes 8388608 | tf_op jit(solution)/shard_map/slice | solution.py:361
  178.7 5.7 %copy.62.refs_13_ = f32[2,4096,128]{2,1,0:T(8,128)} copy(f32[2,4096,128]{1,2,0:T(8,128)} %bitcast.70) | data formatting | bytes 8388608 | tf_op jit(solution)/shard_map/squeeze | solution.py:361
  188.1 57.1 %all-gather.12.cloned.1.call-done = bf16[16384,256]{1,0:T(8,128)(2,1)} async-done(((bf16[1024,256]{1,0:T(8,128)(2,1)}), bf16[16384,256]{1,0:T(8,128)(2,1)}) %all-gather.12.cloned.1.call-update) | async-done | bytes 8388624 | tf_op jit(solution)/shard_map/all_gather | solution.py:373
  245.2 35.1 %mix.3 = (bf16[1024,128]{1,0:T(8,128)(2,1)}, f32[2,4096,128]{2,1,0:T(8,128)}, f32[1024,1]{1,0:T(8,128)}) custom-call(bf16[16,1024,256]{2,1,0:T(8,128)(2,1)} %all-gather.8.cloned.1.call-done.refs_0_, bf16[16,1024,256]{2,1,0:T(8,128)(2,1)} %bitcast.82, f32[16,1,256]{2,1,0:T(1,128)} %bitcast.75, f32[16,1,256]{2,1,0:T(1,128)} %bitcast.76, ...), custom_call_target="tpu_custom_call" | custom-call | flops 20000000000 | bytes 14000000 | tf_op jit(solution)/shard_map/mix/pallas_call | solution.py:214
  280.3 49.1 %all-gather.14.cloned.1.call-done = bf16[16384,128]{1,0:T(8,128)(2,1)} async-done(((bf16[1024,128]{1,0:T(8,128)(2,1)}), bf16[16384,128]{1,0:T(8,128)(2,1)}) %all-gather.14.cloned.1.call-update) | async-done | bytes 4194320 | tf_op jit(solution)/shard_map/all_gather | solution.py:370
  329.4 5.2 %out_proj.3 = (bf16[1024,256]{1,0:T(8,128)(2,1)}, f32[1024,1]{1,0:T(8,128)}) custom-call(bf16[16,1024,128]{2,1,0:T(8,128)(2,1)} %bitcast.84, bf16[2048,256]{1,0:T(8,128)(2,1)} %get-tuple-element.26.w_ref), custom_call_target="tpu_custom_call" | custom-call | flops 4000000000 | bytes 4000000 | tf_op jit(solution)/shard_map/out_proj/pallas_call | solution.py:252
  337.6 3.1 collective-permute-done.1
  340.7 1.5 collective-permute-start.2
  342.3 5.6 %copy.63 = f32[2,4096,128]{1,2,0:T(8,128)} copy(f32[2,4096,128]{2,1,0:T(8,128)} %get-tuple-element.16) | data formatting | bytes 8388608 | tf_op jit(solution)/shard_map/mix/pallas_call | solution.py:214
  347.9 5.6 %copy.64 = f32[2,4096,128]{1,2,0:T(8,128)} copy(f32[2,4096,128]{2,1,0:T(8,128)} %get-tuple-element.17) | data formatting | bytes 8388608 | tf_op jit(solution)/shard_map/mix/pallas_call | solution.py:214
  354.5 7.9 %maximum_bitcast_fusion = f32[2,2,64,2,4096]{4,2,3,1,0:T(8,128)} fusion(f32[1,2,4096,2,64]{2,4,3,1,0:T(8,128)} %bitcast.72, f32[1,2,4096,2,64]{2,4,3,1,0:T(8,128)} %bitcast.71), kind=kLoop, calls=%fused_computation | loop fusion | flops 2097152 | bytes 16777216 | tf_op jit(solution)/shard_map/transpose | solution.py:378
  362.6 3.9 %copy.65 = f32[2,2,64,2,4096]{4,2,1,3,0:T(8,128)S(1)} copy(f32[2,2,64,2,4096]{4,2,3,1,0:T(8,128)} %maximum_bitcast_fusion) | data formatting | bytes 16777216 | tf_op jit(solution)/shard_map/transpose | solution.py:378
  366.6 9.9 %copy.66 = f32[2,128,2,4096]{3,2,1,0:T(2,128)} copy(f32[2,128,2,4096]{3,1,2,0:T(8,128)S(1)} %bitcast.68) | data formatting | bytes 16777216
  (86 shorter events, 19.8 us)
Async XLA Ops:
  7.2 80.0 %all-gather.8.cloned.1.call-start = ((), (), s32[]{:S(2)}) async-start(), calls=%async_computation | async-start | bytes 8912896 | tf_op jit(solution)/shard_map/all_gather | solution.py:348
  7.9 159.1 %all-gather.10.cloned.1.call-start = ((), (), s32[]{:S(2)}) async-start(), calls=%async_computation.1 | async-start | bytes 4456448 | tf_op jit(solution)/shard_map/all_gather | solution.py:370
  24.0 6.0 %copy-start.11 = (f32[2,128]{1,0:T(2,128)S(1)}, f32[2,128]{1,0:T(2,128)}, u32[]{:S(2)}) copy-start(f32[2,128]{1,0:T(2,128)} %param.26) | copy-start | bytes 3076
  24.0 7.1 %copy-start.9 = (f32[2,128,8,2]{1,3,2,0:T(2,128)S(1)}, f32[2,128,8,2]{1,3,2,0:T(2,128)}, u32[]{:S(2)}) copy-start(f32[2,128,8,2]{1,3,2,0:T(2,128)} %param.25) | copy-start | bytes 49156
  24.0 7.9 %copy-start.12 = (f32[2,2]{1,0:T(2,128)S(1)}, f32[2,2]{1,0:T(2,128)}, u32[]{:S(2)}) copy-start(f32[2,2]{1,0:T(2,128)} %param.23) | copy-start | bytes 52
  24.0 8.6 %copy-start.13 = (f32[2,2]{1,0:T(2,128)S(1)}, f32[2,2]{1,0:T(2,128)}, u32[]{:S(2)}) copy-start(f32[2,2]{1,0:T(2,128)} %param.24) | copy-start | bytes 52
  24.0 10.5 %copy-start.8 = (f32[2,4096]{1,0:T(2,128)S(1)}, f32[2,4096]{1,0:T(2,128)}, u32[]{:S(2)}) copy-start(f32[2,4096]{1,0:T(2,128)} %param.16) | copy-start | bytes 98308
  24.1 11.1 %copy-start.3 = (bf16[2,4096,128]{2,1,0:T(8,128)(2,1)S(1)}, bf16[2,4096,128]{2,1,0:T(8,128)(2,1)}, u32[]{:S(2)}) copy-start(bf16[2,4096,128]{2,1,0:T(8,128)(2,1)} %param.20) | copy-start | bytes 6291460
  35.2 3.8 copy-start.4
  35.2 3.8 copy-start.5
  87.2 30.8 %copy-start.2 = (bf16[2,2048,256]{2,1,0:T(8,128)(2,1)S(1)}, bf16[2,2048,256]{2,1,0:T(8,128)(2,1)}, u32[]{:S(2)}) copy-start(bf16[2,2048,256]{2,1,0:T(8,128)(2,1)} %param.27) | copy-start | bytes 6291460
  117.9 127.3 %all-gather.12.cloned.1.call-start = ((), (), s32[]{:S(2)}) async-start(), calls=%async_computation.2 | async-start | bytes 8912896 | tf_op jit(solution)/shard_map/all_gather | solution.py:373
  172.2 157.2 %all-gather.14.cloned.1.call-start = ((), (), s32[]{:S(2)}) async-start(), calls=%async_computation.3 | async-start | bytes 4456448 | tf_op jit(solution)/shard_map/all_gather | solution.py:370
  178.7 8.8 %copy-start.10 = (f32[2,4096]{1,0:T(2,128)S(1)}, f32[2,4096]{1,0:T(2,128)}, u32[]{:S(2)}) copy-start(f32[2,4096]{1,0:T(2,128)} %param.28) | copy-start | bytes 98308
  335.9 1.2 collective-permute-start
  337.1 3.6 collective-permute-start.1
  340.7 12.9 %collective-permute-start.2 = (f32[1024]{0:T(1024)S(1)}, f32[1024]{0:T(1024)S(1)}, u32[]{:S(2)}, u32[]{:S(2)}) collective-permute-start(f32[1024]{0:T(1024)S(1)} %add.41), channel_id=1, source_target_pairs={{0,4},{1,5},{2,6},{3,7},{4,0},{5,1},{6,2},{7,3},{8,12},{9,13},{10,... | collective-permute-start | bytes 12296 | tf_op jit(solution)/shard_map/ppermute | solution.py:282
  353.6 22.9 %collective-permute-start.3 = (f32[1024]{0:T(1024)S(1)}, f32[1024]{0:T(1024)S(1)}, u32[]{:S(2)}, u32[]{:S(2)}) collective-permute-start(f32[1024]{0:T(1024)S(1)} %add.42), channel_id=1, source_target_pairs={{0,8},{1,9},{2,10},{3,11},{4,12},{5,13},{6,14},{7,15},{8,0},{9,1},... | collective-permute-start | bytes 12296 | tf_op jit(solution)/shard_map/ppermute | solution.py:282
  354.5 7.9 %copy-start.7 = (f32[1024,1]{1,0:T(8,128)S(1)}, f32[1024,1]{1,0:T(8,128)}, u32[]{:S(2)}) copy-start(f32[1024,1]{1,0:T(8,128)} %get-tuple-element.12) | copy-start | bytes 12292
  366.6 9.9 %copy-start = (bf16[128,8,256]{2,1,0:T(8,128)(2,1)S(1)}, bf16[128,8,256]{2,1,0:T(8,128)(2,1)}, u32[]{:S(2)}) copy-start(bf16[128,8,256]{2,1,0:T(8,128)(2,1)} %param.15) | copy-start | bytes 1572868
  366.6 9.9 %copy-start.1 = (bf16[1024,256]{1,0:T(8,128)(2,1)S(1)}, bf16[1024,256]{1,0:T(8,128)(2,1)}, u32[]{:S(2)}) copy-start(bf16[1024,256]{1,0:T(8,128)(2,1)} %get-tuple-element.11) | copy-start | bytes 1572868
  366.6 9.9 %copy-start.6 = (bf16[1024,256]{1,0:T(8,128)(2,1)S(1)}, bf16[1024,256]{1,0:T(8,128)(2,1)}, u32[]{:S(2)}) copy-start(bf16[1024,256]{1,0:T(8,128)(2,1)} %get-tuple-element.14) | copy-start | bytes 1572868
Sparse Core Ops, SparseCore 0:
  10.1 77.0 all-gather.7
  118.0 48.9 all-gather.9
  172.4 72.8 all-gather.11
  280.4 48.9 all-gather.13
